TPU v7x, 32 devices: a whole 2x2x4 slice. The times are simulated.
32 devices in a mesh: grp: 2 (over y), ra: 4 (over z), cb: 4 (over x, core).
Axes of the slice: x: 2, y: 2, z: 4, core: 2. Of those that a mesh axis runs over, the one named last changes fastest.
Arguments:
- tokens: bfloat16 [256, 2048], P('grp', 'ra'), parts along dimension 0, may hold values from -8 to 8
- first_gain: bfloat16 [2048], P('ra'), may hold values from 0.099609375 to 1.8984375
- first_gate: bfloat16 [2048, 5632], P('ra', 'cb'), may hold values from -0.125 to 0.125
- first_up: bfloat16 [2048, 5632], P('ra', 'cb'), may hold values from -0.125 to 0.125
- first_down: bfloat16 [5632, 2048], P('cb', 'ra'), may hold values from -0.078125 to 0.078125
- second_gain: bfloat16 [2048], P('ra'), may hold values from 0.099609375 to 1.8984375
- second_gate: bfloat16 [2048, 5632], P('ra', 'cb'), may hold values from -0.125 to 0.125
- second_up: bfloat16 [2048, 5632], P('ra', 'cb'), may hold values from -0.125 to 0.125
- second_down: bfloat16 [5632, 2048], P('cb', 'ra'), may hold values from -0.078125 to 0.078125
Outputs:
- latent_out: bfloat16 [256, 2048], P('grp', 'ra'), parts along dimension 0
There are 2 independent parts, one for each index of `grp`. A program takes and returns all parts, laid end to end along the dimension named above; an argument that names none is the same for every part. Nothing has to cross between parts.
All inputs are finite; a program needn't handle non-finite values.
Results may differ from a plain program's by a relative error of at most 0.0088.
Values may be sent and summed in bfloat16 or wider, within the bound.
No kernel may reach another device: no remote copies, remote signals or barrier semaphores. Data moves between devices by JAX's collectives and lax.ppermute only.
A program may use at most 64 MiB of HBM per device.

v0:
```python
import jax
import jax.numpy as jnp
from jax import lax
from jax.sharding import PartitionSpec as P


def sublayer(x, gain, w_gate, w_up, w_down):
    xf = x.astype(jnp.float32)
    width = x.shape[1] * lax.axis_size("ra")
    rows = x.shape[0]
    squares = jnp.sum(xf * xf, axis=1)
    normed = (xf * gain.astype(jnp.float32)).astype(jnp.bfloat16)
    dims = (((0,), (1,)), ((), ()))
    gate_rows = lax.dot_general(w_gate, normed, dims, preferred_element_type=jnp.float32)
    up_rows = lax.dot_general(w_up, normed, dims, preferred_element_type=jnp.float32)
    shares = lax.psum_scatter(
        jnp.concatenate([gate_rows, up_rows], axis=1), "ra", scatter_dimension=0, tiled=True
    )
    total_sq = lax.psum(squares, "ra")
    scale = lax.rsqrt(total_sq / width + 1e-06)
    hidden_t = (
        jax.nn.silu(shares[:, :rows] * scale[None, :]) * (shares[:, rows:] * scale[None, :])
    ).astype(jnp.bfloat16)
    partial_value = lax.dot_general(
        lax.all_gather(hidden_t, "ra", axis=0, tiled=True),
        w_down,
        (((0,), (0,)), ((), ())),
        preferred_element_type=jnp.float32,
    )
    branch = lax.psum(partial_value, "cb")
    return (0.5 * xf + 0.5 * branch).astype(jnp.bfloat16)


def per_device(
    tokens,
    first_gain,
    first_gate,
    first_up,
    first_down,
    second_gain,
    second_gate,
    second_up,
    second_down,
):
    middle = sublayer(tokens, first_gain, first_gate, first_up, first_down)
    return sublayer(middle, second_gain, second_gate, second_up, second_down)


def solution(mesh):
    placed = (
        P("grp", "ra"),
        P("ra"),
        P("ra", "cb"),
        P("ra", "cb"),
        P("cb", "ra"),
        P("ra"),
        P("ra", "cb"),
        P("ra", "cb"),
        P("cb", "ra"),
    )
    return jax.shard_map(
        per_device, mesh=mesh, in_specs=placed, out_specs=P("grp", "ra"), check_vma=False
    )
```

profile of v0, /device:TPU:0, one launch (start us, length us, event | category | flops | bytes accessed | tf_op | source)
XLA Modules:
  0.0 194.4 jit_solution(9216063514448310554)
XLA Ops:
  6.5 0.0 copy-start
  6.5 0.0 reduce-scatter.7.cloned.1.call-start
  6.5 0.8 convert_element_type.31
  7.4 0.5 copy-done
  7.9 1.3 convolution_bitcast_fusion.2
  9.2 0.0 copy-done.1
  9.2 0.0 copy-done.2
  9.2 0.4 convolution_bitcast_fusion.3
  9.6 0.1 pad_maximum_fusion
  9.7 1.6 copy.12
  11.3 0.0 reduce-scatter.7.cloned.1.call-update
  11.3 0.0 copy-start.3
  11.3 0.0 all-reduce.3.cloned.1.call-start
  11.3 0.1 fusion.1
  11.5 13.6 %psum.28 = f32[128]{0:T(128)S(1)} all-reduce(f32[128]{0:T(128)S(1)} %fusion.1), channel_id=1, replica_groups=mesh['grp'=2,'ra'=4,'cb'=4] {'ra'}, use_global_device_ids=true, to_apply=%region_2.0 | all-reduce | flops 128 | bytes 1024 | tf_op jit(solution)/shard_map/psum | solution.py:19
  25.1 22.5 %reduce-scatter.7.cloned.1.call-done = f32[352,256]{1,0:T(8,128)} async-done(((f32[1408,256]{1,0:T(8,128)}), f32[352,256]{1,0:T(8,128)}) %reduce-scatter.7.cloned.1.call-update) | async-done | bytes 360464
  47.6 1.7 fusion.14
  49.3 0.1 copy.16
  49.4 1.1 copy.17
  50.5 0.1 multiply_convert_fusion.1
  50.6 0.0 copy-start.6
  50.6 0.1 copy.10
  50.8 15.0 %all_gather.6 = bf16[1408,128]{1,0:T(8,128)(2,1)S(1)} all-gather(bf16[352,128]{1,0:T(8,128)(2,1)S(1)} %copy.10), channel_id=1, replica_groups=mesh['grp'=2,'ra'=4,'cb'=4] {'ra'}, dimensions={0}, use_global_device_ids=true | all-gather | bytes 450560 | tf_op jit(solution)/shard_map/all_gather | solution.py:25
  65.8 1.1 fusion.15
  66.9 0.0 all-reduce.3.cloned.1.call-update
  66.9 0.0 copy-start.4
  66.9 0.0 reduce-scatter.9.cloned.1.call-start
  67.0 30.7 %all-reduce.3.cloned.1.call-done = f32[128,512]{1,0:T(8,128)} async-done(((f32[128,512]{1,0:T(8,128)}), f32[128,512]{1,0:T(8,128)}) %all-reduce.3.cloned.1.call-update) | async-done | bytes 262160 | tf_op jit(solution)/shard_map/psum | solution.py:30
  97.7 1.1 fusion.5
  98.8 1.7 convolution_bitcast_fusion
  100.5 0.4 convolution_bitcast_fusion.1
  100.9 0.1 pad_maximum_fusion.1
  101.0 1.6 copy.14
  102.6 0.0 reduce-scatter.9.cloned.1.call-update
  102.6 0.0 copy-start.5
  102.6 0.0 all-reduce.5.cloned.1.call-start
  102.6 12.1 %psum.30 = f32[128]{0:T(128)S(1)} all-reduce(f32[128]{0:T(128)S(1)} %get-tuple-element.5), channel_id=1, replica_groups=mesh['grp'=2,'ra'=4,'cb'=4] {'ra'}, use_global_device_ids=true, to_apply=%region_6.7 | all-reduce | flops 128 | bytes 1024 | tf_op jit(solution)/shard_map/psum | solution.py:19
  114.7 21.5 %reduce-scatter.9.cloned.1.call-done = f32[352,256]{1,0:T(8,128)} async-done(((f32[1408,256]{1,0:T(8,128)}), f32[352,256]{1,0:T(8,128)}) %reduce-scatter.9.cloned.1.call-update) | async-done | bytes 360464
  136.2 1.7 fusion.13
  137.9 0.1 copy.18
  138.0 1.1 copy.19
  139.1 0.1 multiply_convert_fusion
  139.2 0.1 copy.11
  139.3 15.1 %all_gather.7 = bf16[1408,128]{1,0:T(8,128)(2,1)S(1)} all-gather(bf16[352,128]{1,0:T(8,128)(2,1)S(1)} %copy.11), channel_id=1, replica_groups=mesh['grp'=2,'ra'=4,'cb'=4] {'ra'}, dimensions={0}, use_global_device_ids=true | all-gather | bytes 450560 | tf_op jit(solution)/shard_map/all_gather | solution.py:25
  154.4 1.1 fusion.16
  155.5 0.0 all-reduce.5.cloned.1.call-update
  155.5 30.7 %all-reduce.5.cloned.1.call-done = f32[128,512]{1,0:T(8,128)} async-done(((f32[128,512]{1,0:T(8,128)}), f32[128,512]{1,0:T(8,128)}) %all-reduce.5.cloned.1.call-update) | async-done | bytes 262160 | tf_op jit(solution)/shard_map/psum | solution.py:30
  186.2 1.6 fusion.7
  (9 shorter events, 0.0 us)
Async XLA Ops:
  6.5 1.4 copy-start
  6.5 2.7 %copy-start.1 = (bf16[128,512]{1,0:T(8,128)(2,1)S(1)}, bf16[128,512]{1,0:T(8,128)(2,1)}, u32[]{:S(2)}) copy-start(bf16[128,512]{1,0:T(8,128)(2,1)} %param.9) | copy-start | bytes 393220
  6.5 2.7 %copy-start.2 = (bf16[512,1408]{1,0:T(8,128)(2,1)S(1)}, bf16[512,1408]{1,0:T(8,128)(2,1)}, u32[]{:S(2)}) copy-start(bf16[512,1408]{1,0:T(8,128)(2,1)} %param.11) | copy-start | bytes 4325380
  6.5 41.1 %reduce-scatter.7.cloned.1.call-start = ((), (), s32[]{:S(2)}) async-start(), calls=%async_computation.4 | async-start | bytes 1802240
  11.3 54.5 %copy-start.3 = (bf16[1408,512]{1,0:T(8,128)(2,1)S(1)}, bf16[1408,512]{1,0:T(8,128)(2,1)}, u32[]{:S(2)}) copy-start(bf16[1408,512]{1,0:T(8,128)(2,1)} %param.13) | copy-start | bytes 4325380
  11.3 86.4 %all-reduce.3.cloned.1.call-start = ((), (), s32[]{:S(2)}) async-start(), calls=%async_computation.2 | async-start | bytes 524288 | tf_op jit(solution)/shard_map/psum | solution.py:30
  50.6 16.3 %copy-start.6 = (bf16[512]{0:T(512)(128)(2,1)S(1)}, bf16[512]{0:T(512)(128)(2,1)}, u32[]{:S(2)}) copy-start(bf16[512]{0:T(512)(128)(2,1)} %param.14) | copy-start | bytes 3076
  66.9 33.6 %copy-start.4 = (bf16[512,1408]{1,0:T(8,128)(2,1)S(1)}, bf16[512,1408]{1,0:T(8,128)(2,1)}, u32[]{:S(2)}) copy-start(bf16[512,1408]{1,0:T(8,128)(2,1)} %param.15) | copy-start | bytes 4325380
  66.9 69.3 %reduce-scatter.9.cloned.1.call-start = ((), (), s32[]{:S(2)}) async-start(), calls=%async_computation.5 | async-start | bytes 1802240
  102.6 51.8 %copy-start.5 = (bf16[1408,512]{1,0:T(8,128)(2,1)S(1)}, bf16[1408,512]{1,0:T(8,128)(2,1)}, u32[]{:S(2)}) copy-start(bf16[1408,512]{1,0:T(8,128)(2,1)} %param.17) | copy-start | bytes 4325380
  102.6 83.6 %all-reduce.5.cloned.1.call-start = ((), (), s32[]{:S(2)}) async-start(), calls=%async_computation.3 | async-start | bytes 524288 | tf_op jit(solution)/shard_map/psum | solution.py:30
Sparse Core Ops, SparseCore 0:
  11.4 36.1 reduce-scatter.6
  67.0 30.5 all-reduce.2
  102.7 33.4 reduce-scatter.8
  155.7 30.5 all-reduce.4
where the time goes:
time: 195 us; the launch traced here: 194 us
  waiting for transfers between devices  105 us (54%)
  blocking collectives  55.8 us (29%)
  between operations  13.3 us (7%)
  local copies, waits for them, and re-layouts  9.67 us (5%)
  matrix products  6.01 us (3%)
  other arithmetic  4.14 us (2%)
    psum x2, waiting for transfers between devices, sublayer(): branch = lax.psum(partial_value, 'cb')  61.4 us
    unnamed x6, waiting for transfers between devices  44 us
    all_gather x2, blocking collectives, sublayer(): lax.all_gather(hidden_t, 'ra', axis=0, tiled=True)  30.1 us
    psum x2, blocking collectives, sublayer(): total_sq = lax.psum(squares, 'ra')  25.7 us
    unnamed x20, local copies, waits for them, and re-layouts  6.04 us
  transfers between devices with their start and end apart: 4, of which 4 were waited for; matrix products, arithmetic and copies ran while one was open for 0% of the time, Pallas kernels for 0%

commit v1 on v0

--- a/solution.py
+++ b/solution.py
@@ -27,7 +27,10 @@
         (((0,), (0,)), ((), ())),
         preferred_element_type=jnp.float32,
     )
-    branch = lax.psum(partial_value, "cb")
+    count, branch = (lax.axis_size("cb"), partial_value)
+    for stride in [1 << k for k in range(count.bit_length() - 1)]:
+        swap = [(i, i ^ stride) for i in range(count)]
+        branch = branch + lax.ppermute(branch, "cb", swap)
     return (0.5 * xf + 0.5 * branch).astype(jnp.bfloat16)
 
 

time: 195 us -> 147 us (0.75)
  waiting for transfers between devices: 105 us -> 62.1 us
  starting transfers between devices: 0.13 us -> 3.33 us
  blocking collectives: 55.8 us -> 52.7 us
  matrix products: 6.01 us -> 3.24 us
    psum x2 -> x0, waiting for transfers between devices: 61.4 us -> none  [sublayer(): branch = lax.psum(partial_value, 'cb')]
    ppermute x0 -> x4, waiting for transfers between devices: none -> 16.7 us  [sublayer(): branch = branch + lax.ppermute(branch, 'cb', swap)]
    ppermute x0 -> x4, starting transfers between devices: none -> 3.29 us  [sublayer(): branch = branch + lax.ppermute(branch, 'cb', swap)]
    psum x2, blocking collectives: 25.7 us -> 22.7 us  [sublayer(): total_sq = lax.psum(squares, 'ra')]
    unnamed x6 -> x4, waiting for transfers between devices: 44 us -> 45.4 us
    unnamed x20 -> x22, local copies, waits for them, and re-layouts: 6.04 us -> 6.07 us
  transfers between devices with their start and end apart: 4 -> 6, of which waited for: 4 -> 6; matrix products, arithmetic and copies ran while one was open for 0% -> 0% of each run, Pallas kernels for 0% -> 0%
where the time goes in v1:
time: 147 us
  waiting for transfers between devices  62.1 us (42%)
  blocking collectives  52.7 us (36%)
  between operations  13.6 us (9%)
  local copies, waits for them, and re-layouts  9.7 us (7%)
  starting transfers between devices  3.33 us (2%)
  matrix products  3.24 us (2%)
  other arithmetic  2.36 us (2%)
    unnamed x4, waiting for transfers between devices  45.4 us
    all_gather x2, blocking collectives, sublayer(): lax.all_gather(hidden_t, 'ra', axis=0, tiled=True)  30 us
    psum x2, blocking collectives, sublayer(): total_sq = lax.psum(squares, 'ra')  22.7 us
    ppermute x4, waiting for transfers between devices, sublayer(): branch = branch + lax.ppermute(branch, 'cb', swap)  16.7 us
    unnamed x22, local copies, waits for them, and re-layouts  6.07 us
    slice x2, local copies, waits for them, and re-layouts, sublayer(): shares[:, :rows] * scale[None, :]  3.39 us
    ppermute x4, starting transfers between devices, sublayer(): branch = branch + lax.ppermute(branch, 'cb', swap)  3.29 us
  transfers between devices with their start and end apart: 6, of which 6 were waited for; matrix products, arithmetic and copies ran while one was open for 0% of the time, Pallas kernels for 0%

profile of v1, /device:TPU:0, one launch (start us, length us, event | category | flops | bytes accessed | tf_op | source)
XLA Modules:
  0.0 147.0 jit_solution(14852452782660373370)
XLA Ops:
  6.5 0.0 copy-start
  6.5 0.0 reduce-scatter.7.cloned.1.call-start
  6.5 0.8 convert_element_type.31
  7.4 0.5 copy-done
  7.9 1.3 convolution_bitcast_fusion.2
  9.2 0.4 convolution_bitcast_fusion.3
  9.6 0.1 pad_maximum_fusion
  9.7 1.6 %copy.12 = f32[1408,256]{1,0:T(8,128)} copy(f32[1408,256]{0,1:T(8,128)S(1)} %pad_maximum_fusion) | data formatting | bytes 2883584
  11.3 0.0 reduce-scatter.7.cloned.1.call-update
  11.3 0.0 copy-start.3
  11.3 0.0 reduce-scatter.9.cloned.1.call-start
  11.4 0.1 fusion.1
  11.5 13.6 %psum.14 = f32[128]{0:T(128)S(1)} all-reduce(f32[128]{0:T(128)S(1)} %fusion.1), channel_id=1, replica_groups=mesh['grp'=2,'ra'=4,'cb'=4] {'ra'}, use_global_device_ids=true, to_apply=%region_2.0 | all-reduce | flops 128 | bytes 1024 | tf_op jit(solution)/shard_map/psum | solution.py:19
  25.1 22.5 %reduce-scatter.7.cloned.1.call-done = f32[352,256]{1,0:T(8,128)} async-done(((f32[1408,256]{1,0:T(8,128)}), f32[352,256]{1,0:T(8,128)}) %reduce-scatter.7.cloned.1.call-update) | async-done | bytes 360464
  47.6 1.7 %fusion.14 = (f32[352,128]{1,0:T(8,128)S(1)}, f32[352,128]{1,0:T(8,128)}) fusion(f32[352,256]{1,0:T(8,128)} %reduce-scatter.7.cloned.1.call-done), kind=kLoop, calls=%fused_computation.25 | loop fusion | bytes 720896 | tf_op jit(solution)/shard_map/slice | solution.py:22
  49.3 0.1 copy.16
  49.4 1.1 copy.17
  50.5 0.1 multiply_convert_fusion.1
  50.6 0.1 copy.10
  50.8 15.0 %all_gather.6 = bf16[1408,128]{1,0:T(8,128)(2,1)S(1)} all-gather(bf16[352,128]{1,0:T(8,128)(2,1)S(1)} %copy.10), channel_id=1, replica_groups=mesh['grp'=2,'ra'=4,'cb'=4] {'ra'}, dimensions={0}, use_global_device_ids=true | all-gather | bytes 450560 | tf_op jit(solution)/shard_map/all_gather | solution.py:25
  65.8 0.4 fusion.15
  66.2 0.1 collective-permute-start
  66.3 1.5 %collective-permute-done = f32[128,512]{1,0:T(8,128)S(1)} collective-permute-done((f32[128,512]{1,0:T(8,128)S(1)}, f32[128,512]{1,0:T(8,128)S(1)}, u32[]{:S(2)}, u32[]{:S(2)}) %collective-permute-start) | collective-permute-done | bytes 262176 | tf_op jit(solution)/shard_map/ppermute | solution.py:33
  67.8 1.6 %collective-permute-start.1 = (f32[128,512]{1,0:T(8,128)S(1)}, f32[128,512]{1,0:T(8,128)S(1)}, u32[]{:S(2)}, u32[]{:S(2)}) collective-permute-start(f32[128,512]{1,0:T(8,128)S(1)} %add.43), channel_id=1, source_target_pairs={{0,2},{1,3},{2,0},{3,1},{4,6},{5,7},{6,4},{7,5},{8,10},{9,11},{10,... | collective-permute-start | bytes 786440 | tf_op jit(solution)/shard_map/ppermute | solution.py:33
  69.4 0.0 copy-done.7
  69.4 6.8 %collective-permute-done.1 = f32[128,512]{1,0:T(8,128)S(1)} collective-permute-done((f32[128,512]{1,0:T(8,128)S(1)}, f32[128,512]{1,0:T(8,128)S(1)}, u32[]{:S(2)}, u32[]{:S(2)}) %collective-permute-start.1) | collective-permute-done | bytes 262176 | tf_op jit(solution)/shard_map/ppermute | solution.py:33
  76.3 0.1 fusion.5
  76.4 0.4 convolution_bitcast_fusion
  76.8 0.4 convolution_bitcast_fusion.1
  77.2 0.1 pad_maximum_fusion.1
  77.3 1.6 %copy.14 = f32[1408,256]{1,0:T(8,128)} copy(f32[1408,256]{0,1:T(8,128)S(1)} %pad_maximum_fusion.1) | data formatting | bytes 2883584
  78.9 0.0 reduce-scatter.9.cloned.1.call-update
  78.9 0.0 copy-start.6
  78.9 9.0 %psum.15 = f32[128]{0:T(128)S(1)} all-reduce(f32[128]{0:T(128)S(1)} %get-tuple-element.5), channel_id=1, replica_groups=mesh['grp'=2,'ra'=4,'cb'=4] {'ra'}, use_global_device_ids=true, to_apply=%region_5.6 | all-reduce | flops 128 | bytes 1024 | tf_op jit(solution)/shard_map/psum | solution.py:19
  87.9 22.8 %reduce-scatter.9.cloned.1.call-done = f32[352,256]{1,0:T(8,128)} async-done(((f32[1408,256]{1,0:T(8,128)}), f32[352,256]{1,0:T(8,128)}) %reduce-scatter.9.cloned.1.call-update) | async-done | bytes 360464
  110.8 1.7 %fusion.13 = (f32[352,128]{1,0:T(8,128)S(1)}, f32[352,128]{1,0:T(8,128)}) fusion(f32[352,256]{1,0:T(8,128)} %reduce-scatter.9.cloned.1.call-done), kind=kLoop, calls=%fused_computation.24 | loop fusion | bytes 720896 | tf_op jit(solution)/shard_map/slice | solution.py:22
  112.5 0.1 copy.18
  112.6 1.1 copy.19
  113.7 0.1 multiply_convert_fusion
  113.8 0.1 copy.11
  113.9 15.0 %all_gather.7 = bf16[1408,128]{1,0:T(8,128)(2,1)S(1)} all-gather(bf16[352,128]{1,0:T(8,128)(2,1)S(1)} %copy.11), channel_id=1, replica_groups=mesh['grp'=2,'ra'=4,'cb'=4] {'ra'}, dimensions={0}, use_global_device_ids=true | all-gather | bytes 450560 | tf_op jit(solution)/shard_map/all_gather | solution.py:25
  129.0 0.0 copy-done.6
  129.0 0.4 fusion.16
  129.4 0.1 collective-permute-start.2
  129.5 1.5 %collective-permute-done.2 = f32[128,512]{1,0:T(8,128)S(1)} collective-permute-done((f32[128,512]{1,0:T(8,128)S(1)}, f32[128,512]{1,0:T(8,128)S(1)}, u32[]{:S(2)}, u32[]{:S(2)}) %collective-permute-start.2) | collective-permute-done | bytes 262176 | tf_op jit(solution)/shard_map/ppermute | solution.py:33
  131.0 1.6 %collective-permute-start.3 = (f32[128,512]{1,0:T(8,128)S(1)}, f32[128,512]{1,0:T(8,128)S(1)}, u32[]{:S(2)}, u32[]{:S(2)}) collective-permute-start(f32[128,512]{1,0:T(8,128)S(1)} %add.48), channel_id=1, source_target_pairs={{0,2},{1,3},{2,0},{3,1},{4,6},{5,7},{6,4},{7,5},{8,10},{9,11},{10,... | collective-permute-start | bytes 786440 | tf_op jit(solution)/shard_map/ppermute | solution.py:33
  132.6 6.8 %collective-permute-done.3 = f32[128,512]{1,0:T(8,128)S(1)} collective-permute-done((f32[128,512]{1,0:T(8,128)S(1)}, f32[128,512]{1,0:T(8,128)S(1)}, u32[]{:S(2)}, u32[]{:S(2)}) %collective-permute-start.3) | collective-permute-done | bytes 262176 | tf_op jit(solution)/shard_map/ppermute | solution.py:33
  139.4 0.7 fusion.7
  (15 shorter events, 0.1 us)
Async XLA Ops:
  6.5 1.4 copy-start
  6.5 2.7 %copy-start.1 = (bf16[128,512]{1,0:T(8,128)(2,1)S(1)}, bf16[128,512]{1,0:T(8,128)(2,1)}, u32[]{:S(2)}) copy-start(bf16[128,512]{1,0:T(8,128)(2,1)} %param.9) | copy-start | bytes 393220
  6.5 2.7 %copy-start.2 = (bf16[512,1408]{1,0:T(8,128)(2,1)S(1)}, bf16[512,1408]{1,0:T(8,128)(2,1)}, u32[]{:S(2)}) copy-start(bf16[512,1408]{1,0:T(8,128)(2,1)} %param.11) | copy-start | bytes 4325380
  6.5 41.1 %reduce-scatter.7.cloned.1.call-start = ((), (), s32[]{:S(2)}) async-start(), calls=%async_computation.2 | async-start | bytes 1802240
  11.3 54.5 %copy-start.3 = (bf16[1408,512]{1,0:T(8,128)(2,1)S(1)}, bf16[1408,512]{1,0:T(8,128)(2,1)}, u32[]{:S(2)}) copy-start(bf16[1408,512]{1,0:T(8,128)(2,1)} %param.13) | copy-start | bytes 4325380
  11.3 99.5 %reduce-scatter.9.cloned.1.call-start = ((), (), s32[]{:S(2)}) async-start(), calls=%async_computation.3 | async-start | bytes 1802240
  65.8 3.6 %copy-start.7 = (bf16[512]{0:T(512)(128)(2,1)S(1)}, bf16[512]{0:T(512)(128)(2,1)}, u32[]{:S(2)}) copy-start(bf16[512]{0:T(512)(128)(2,1)} %param.14) | copy-start | bytes 3076
  65.8 10.6 %copy-start.4 = (bf16[512,1408]{1,0:T(8,128)(2,1)S(1)}, bf16[512,1408]{1,0:T(8,128)(2,1)}, u32[]{:S(2)}) copy-start(bf16[512,1408]{1,0:T(8,128)(2,1)} %param.16) | copy-start | bytes 4325380
  66.2 1.6 %collective-permute-start = (f32[128,512]{1,0:T(8,128)S(1)}, f32[128,512]{1,0:T(8,128)S(1)}, u32[]{:S(2)}, u32[]{:S(2)}) collective-permute-start(f32[128,512]{1,0:T(8,128)S(1)} %fusion.15), channel_id=1, source_target_pairs={{0,1},{1,0},{2,3},{3,2},{4,5},{5,4},{6,7},{7,6},{8,9},{9,8},{10,11... | collective-permute-start | bytes 786440 | tf_op jit(solution)/shard_map/ppermute | solution.py:33
  67.8 8.4 %collective-permute-start.1 = (f32[128,512]{1,0:T(8,128)S(1)}, f32[128,512]{1,0:T(8,128)S(1)}, u32[]{:S(2)}, u32[]{:S(2)}) collective-permute-start(f32[128,512]{1,0:T(8,128)S(1)} %add.43), channel_id=1, source_target_pairs={{0,2},{1,3},{2,0},{3,1},{4,6},{5,7},{6,4},{7,5},{8,10},{9,11},{10,... | collective-permute-start | bytes 786440 | tf_op jit(solution)/shard_map/ppermute | solution.py:33
  69.4 7.4 %copy-start.5 = (bf16[512,1408]{1,0:T(8,128)(2,1)S(1)}, bf16[512,1408]{1,0:T(8,128)(2,1)}, u32[]{:S(2)}) copy-start(bf16[512,1408]{1,0:T(8,128)(2,1)} %param.15) | copy-start | bytes 4325380
  78.9 50.1 %copy-start.6 = (bf16[1408,512]{1,0:T(8,128)(2,1)S(1)}, bf16[1408,512]{1,0:T(8,128)(2,1)}, u32[]{:S(2)}) copy-start(bf16[1408,512]{1,0:T(8,128)(2,1)} %param.17) | copy-start | bytes 4325380
  129.4 1.6 %collective-permute-start.2 = (f32[128,512]{1,0:T(8,128)S(1)}, f32[128,512]{1,0:T(8,128)S(1)}, u32[]{:S(2)}, u32[]{:S(2)}) collective-permute-start(f32[128,512]{1,0:T(8,128)S(1)} %fusion.16), channel_id=1, source_target_pairs={{0,1},{1,0},{2,3},{3,2},{4,5},{5,4},{6,7},{7,6},{8,9},{9,8},{10,11... | collective-permute-start | bytes 786440 | tf_op jit(solution)/shard_map/ppermute | solution.py:33
  131.0 8.4 %collective-permute-start.3 = (f32[128,512]{1,0:T(8,128)S(1)}, f32[128,512]{1,0:T(8,128)S(1)}, u32[]{:S(2)}, u32[]{:S(2)}) collective-permute-start(f32[128,512]{1,0:T(8,128)S(1)} %add.48), channel_id=1, source_target_pairs={{0,2},{1,3},{2,0},{3,1},{4,6},{5,7},{6,4},{7,5},{8,10},{9,11},{10,... | collective-permute-start | bytes 786440 | tf_op jit(solution)/shard_map/ppermute | solution.py:33
Sparse Core Ops, SparseCore 0:
  11.4 36.1 reduce-scatter.6
  79.0 31.7 reduce-scatter.8
